TPU v7x, 32 devices: a whole 2x2x4 slice. The times are simulated.
32 devices in a mesh: tp: 4 (over y, x), dp: 8 (over z, core).
Axes of the slice: x: 2, y: 2, z: 4, core: 2. Of those that a mesh axis runs over, the one named last changes fastest.
Arguments:
- stream: bfloat16 [16, 4096], P('tp', 'dp'), may hold values from -48 to 48
- norm_gain: float32 [2, 4096], P(None, 'dp'), may hold values from 0.1 to 1.9
- x_weight: bfloat16 [2, 4096, 8192], P(None, 'dp', 'tp'), may hold values from -0.09375 to 0.09375
- z_weight: bfloat16 [2, 4096, 8192], P(None, 'dp', 'tp'), may hold values from -0.09375 to 0.09375
- bc_weight: bfloat16 [2, 4096, 2, 2048], P(None, 'dp', None, 'tp'), may hold values from -0.09375 to 0.09375
- step_weight: bfloat16 [2, 4096, 128], P(None, 'dp'), may hold values from -0.09375 to 0.09375
- conv_x_weight: bfloat16 [2, 5, 8192], P(None, None, 'tp'), may hold values from -2.5 to 2.5
- conv_bc_weight: bfloat16 [2, 5, 2, 2048], P(None, None, None, 'tp'), may hold values from -2.5 to 2.5
- step_bias: float32 [2, 128], P(None, 'tp'), may hold values from -4 to 0.5
- decay_log: float32 [2, 128], P(None, 'tp'), may hold values from 0 to 2.8
- skip_gain: float32 [2, 128], P(None, 'tp'), may hold values from 0.1 to 1.9
- group_gain: float32 [2, 8192], P(None, 'tp'), may hold values from 0.1 to 1.9
- out_weight: bfloat16 [2, 8192, 4096], P(None, 'tp', 'dp'), may hold values from -0.0625 to 0.0625
- scan_state: float32 [2, 16, 128, 64, 128], P(None, 'dp', 'tp'), may hold values from -1.2 to 1.2
- conv_x_state: bfloat16 [2, 16, 4, 8192], P(None, 'dp', None, 'tp'), may hold values from -6 to 6
- conv_bc_state: bfloat16 [2, 16, 4, 2, 2048], P(None, 'dp', None, None, 'tp'), may hold values from -6 to 6
Outputs:
- stream_out: bfloat16 [16, 4096], P('tp', 'dp')
- scan_state_out: float32 [2, 16, 128, 64, 128], P(None, 'dp', 'tp')
- conv_x_out: bfloat16 [2, 16, 4, 8192], P(None, 'dp', None, 'tp')
- conv_bc_out: bfloat16 [2, 16, 4, 2, 2048], P(None, 'dp', None, None, 'tp')
All inputs are finite; a program needn't handle non-finite values.
Results may differ from a plain program's by a relative error of at most 0.04.
Values may be sent and summed in bfloat16 or wider, within the bound.
A program may use at most 64 MiB of HBM per device.

v0:
```python
import jax
import jax.numpy as jnp
from jax import lax
from jax.sharding import PartitionSpec as P

MODEL_WIDTH = 4096
HEAD_COUNT = 128
HEAD_DIM = 64
STATE_DIM = 128
GROUPS = 16
LAYERS = 2


EPS = 1e-06


def shards(
    stream,
    norm_gain,
    x_weight,
    z_weight,
    bc_weight,
    step_weight,
    conv_x_weight,
    conv_bc_weight,
    step_bias,
    decay_log,
    skip_gain,
    group_gain,
    out_weight,
    scan_state,
    conv_x_state,
    conv_bc_state,
):
    tp_index = lax.axis_index("tp")
    dp_index = lax.axis_index("dp")
    seq_count = scan_state.shape[1]
    heads_dev = scan_state.shape[2]
    groups_dev = conv_bc_state.shape[4] // STATE_DIM
    per_group = HEAD_COUNT // GROUPS
    weight_rows = x_weight.shape[1]
    whole = None
    states_list = []
    xconv_list = []
    bcconv_list = []
    for block_index in range(LAYERS):
        if whole is None:
            whole = lax.all_gather(stream, "tp", axis=0, tiled=True)
        widened = whole.astype(jnp.float32)
        normed_in = (widened * norm_gain[block_index]).astype(jnp.bfloat16)
        part_sq = jnp.sum(widened * widened, axis=1)
        step_cols = lax.dynamic_slice_in_dim(
            step_weight[block_index], tp_index * heads_dev, heads_dev, 1
        )
        part_x = jnp.dot(normed_in, x_weight[block_index], preferred_element_type=jnp.float32)
        part_z = jnp.dot(normed_in, z_weight[block_index], preferred_element_type=jnp.float32)
        part_bc = jnp.dot(
            normed_in,
            bc_weight[block_index].reshape(weight_rows, -1),
            preferred_element_type=jnp.float32,
        )
        part_step = jnp.dot(normed_in, step_cols, preferred_element_type=jnp.float32)
        total_sq = lax.psum(part_sq.astype(jnp.bfloat16), "dp").astype(jnp.float32)
        got_sq = lax.dynamic_slice_in_dim(total_sq, dp_index * seq_count, seq_count, 0)
        got_x, got_z, got_bc, got_step = (
            lax.psum_scatter(
                part_x.astype(jnp.bfloat16), "dp", scatter_dimension=0, tiled=True
            ).astype(jnp.float32),
            lax.psum_scatter(
                part_z.astype(jnp.bfloat16), "dp", scatter_dimension=0, tiled=True
            ).astype(jnp.float32),
            lax.psum_scatter(
                part_bc.astype(jnp.bfloat16), "dp", scatter_dimension=0, tiled=True
            ).astype(jnp.float32),
            lax.psum_scatter(
                part_step.astype(jnp.bfloat16), "dp", scatter_dimension=0, tiled=True
            ).astype(jnp.float32),
        )
        inv_rms = lax.rsqrt(got_sq / MODEL_WIDTH + EPS)[:, None]
        proj_x = (got_x * inv_rms).astype(jnp.bfloat16)
        proj_z = (got_z * inv_rms).astype(jnp.bfloat16)
        proj_bc = (got_bc * inv_rms).astype(jnp.bfloat16).reshape(seq_count, 2, -1)
        step_raw = got_step * inv_rms
        window_x = jnp.concatenate([conv_x_state[block_index], proj_x[:, None, :]], axis=1)
        inputs_x = jax.nn.silu(
            jnp.sum(
                window_x.astype(jnp.float32) * conv_x_weight[block_index].astype(jnp.float32),
                axis=1,
            )
        )
        window_bc = jnp.concatenate([conv_bc_state[block_index], proj_bc[:, None]], axis=1)
        inputs_bc = jax.nn.silu(
            jnp.sum(
                window_bc.astype(jnp.float32) * conv_bc_weight[block_index].astype(jnp.float32),
                axis=1,
            )
        )
        b_part = inputs_bc[:, 0].reshape(seq_count, groups_dev, STATE_DIM)
        c_part = inputs_bc[:, 1].reshape(seq_count, groups_dev, STATE_DIM)
        step_size = jax.nn.softplus(step_raw + step_bias[block_index])
        decay_rate = jnp.exp(-step_size * jnp.exp(decay_log[block_index]))
        heads_x = inputs_x.reshape(seq_count, groups_dev, per_group, HEAD_DIM)
        step_heads = step_size.reshape(seq_count, groups_dev, per_group)
        decay_heads = decay_rate.reshape(seq_count, groups_dev, per_group)
        old_state = scan_state[block_index].reshape(
            seq_count, groups_dev, per_group, HEAD_DIM, STATE_DIM
        )
        state_new = (
            old_state * decay_heads[..., None, None]
            + (step_heads[..., None] * heads_x)[..., None] * b_part[:, :, None, None, :]
        )
        readout = jnp.einsum("sgepn,sgn->sgep", state_new, c_part, precision=lax.Precision.HIGHEST)
        readout = (
            readout
            + skip_gain[block_index].reshape(groups_dev, per_group)[None, :, :, None] * heads_x
        )
        gated_out = readout.reshape(seq_count, -1) * jax.nn.silu(proj_z.astype(jnp.float32))
        grouped = gated_out.reshape(seq_count, groups_dev, -1)
        normed = grouped * lax.rsqrt(jnp.mean(grouped * grouped, axis=2, keepdims=True) + EPS)
        mixed_rows = (normed.reshape(seq_count, -1) * group_gain[block_index]).astype(jnp.bfloat16)
        out_block = out_weight[block_index]
        terms = jnp.dot(
            lax.all_gather(mixed_rows, "dp", axis=0, tiled=True),
            out_block,
            preferred_element_type=jnp.float32,
        )
        summed = lax.psum(terms.astype(jnp.bfloat16), "tp").astype(jnp.float32)
        whole = (widened + summed).astype(jnp.bfloat16)
        states_list.append(state_new.reshape(seq_count, heads_dev, HEAD_DIM, STATE_DIM))
        xconv_list.append(window_x[:, 1:])
        bcconv_list.append(window_bc[:, 1:])
    row_share = stream.shape[0]
    result = lax.dynamic_slice_in_dim(whole, tp_index * row_share, row_share, 0)
    return (result, jnp.stack(states_list), jnp.stack(xconv_list), jnp.stack(bcconv_list))


def solution(mesh):
    in_specs = (
        P("tp", "dp"),
        P(None, "dp"),
        P(None, "dp", "tp"),
        P(None, "dp", "tp"),
        P(None, "dp", None, "tp"),
        P(None, "dp", None),
        P(None, None, "tp"),
        P(None, None, None, "tp"),
        P(None, "tp"),
        P(None, "tp"),
        P(None, "tp"),
        P(None, "tp"),
        P(None, "tp", "dp"),
        P(None, "dp", "tp", None, None),
        P(None, "dp", None, "tp"),
        P(None, "dp", None, None, "tp"),
    )
    out_specs = (
        P("tp", "dp"),
        P(None, "dp", "tp", None, None),
        P(None, "dp", None, "tp"),
        P(None, "dp", None, None, "tp"),
    )
    return jax.shard_map(shards, mesh=mesh, in_specs=in_specs, out_specs=out_specs, check_vma=False)
```

profile of v0, /device:TPU:0, one launch (start us, length us, event | category | flops | bytes accessed | tf_op | source)
XLA Modules:
  0.0 266.7 jit_solution(1172160447030568717)
XLA Ops:
  7.2 1.3 fusion.71
  8.5 9.8 %all-gather = bf16[4,4,512]{2,1,0:T(4,128)(2,1)S(1)} all-gather(bf16[1,4,512]{2,1,0:T(4,128)(2,1)} %bitcast.160), channel_id=1, replica_groups=mesh['tp'=4,'dp'=8] {'tp'}, dimensions={0}, use_global_device_ids=true | all-gather | bytes 20480 | tf_op jit(solution)/shard_map/all_gather | solution.py:48
  18.5 2.6 convolution_convert_fusion.3
  21.1 2.6 convolution_convert_fusion.2
  23.8 0.7 copy-done.16
  24.5 0.6 bitcast_convert_fusion
  25.4 2.2 fusion.67
  28.8 27.7 %all-reduce.9 = (bf16[16]{0:T(256)(128)(2,1)S(1)}, bf16[16,1024]{1,0:T(8,128)(2,1)S(1)}, bf16[16,32]{1,0:T(8,128)(2,1)S(1)}) all-reduce(bf16[16]{0:T(256)(128)(2,1)S(1)} %get-tuple-element.40, bf16[16,1024]{1,0:T(8,128)(2,1)S(1)} %convolution_convert_fusion.5, ...), channel_id=1, replica_groups=mesh['tp'=4,'dp'=8] {'dp'}, use_global_device_ids=true, to_apply=%region_2.0 | all-reduce | flops 16912 | bytes 67648 | tf_op jit(solution)/shard_map/psum | solution.py:63
  56.6 0.6 dynamic-slice.2
  58.1 0.6 exponential_bitcast_fusion
  59.4 0.7 mul.431
  60.1 0.7 fusion.69
  60.7 0.7 mul.428
  61.4 0.7 mul.452
  62.1 0.6 fusion.70
  62.7 0.6 broadcast_bitcast_fusion.1
  63.3 1.5 copy.44
  64.8 0.7 mul.499
  65.5 0.8 fusion.42
  66.3 0.6 fusion.53
  67.0 12.3 %all-reduce.17.cloned.1.call-done = (bf16[16,2048]{1,0:T(8,128)(2,1)}, bf16[16,2048]{1,0:T(8,128)(2,1)}) async-done(((bf16[16,2048]{1,0:T(8,128)(2,1)}, bf16[16,2048]{1,0:T(8,128)(2,1)}), (bf16[16,2048]{1,0:T(8,128)(2,1)}, bf16[16,2048]{1,0:T(8,128)(2,1)})) %all-reduce.17.cloned.1.call-update) | async-done | bytes 131088
  79.2 0.8 fusion.58
  80.7 0.7 multiply_reduce_fusion.1
  81.4 0.8 reduce_sum.82
  82.2 1.4 reduce_sum.90
  83.6 0.7 broadcast_multiply_fusion.1
  84.3 6.0 %fusion.17 = f32[2,4,1,8,64]{4,2,3,1,0:T(1,128)S(1)} fusion(f32[2,4,8,64,128]{4,3,2,1,0:T(8,128)S(1)} %bitcast.138, f32[2,4,128]{2,1,0:T(4,128)} %bitcast.149, f32[2,4,8,64]{3,2,1,0:T(8,128)S(1)} %broadcast_multiply_fusion.1, f32[2,4,8]{2,1,0:T(4,128)} %mul.428, f32[2,2,512]{2,1,0:T(2,128)} %copy-done.10), kind=kOutput, calls=%fused_computation.24 | convolution fusion | flops 7864320 | bytes 2142208 | tf_op jit(solution)/shard_map/sgepn,sgn->sgep/dot_general | solution.py:112
  90.3 0.8 multiply_add_fusion.3
  91.2 0.9 fusion.65
  92.3 0.7 fusion.55
  93.0 14.0 %all-gather.1 = bf16[8,2,2048]{2,1,0:T(2,128)(2,1)S(1)} all-gather(bf16[1,2,2048]{2,1,0:T(2,128)(2,1)S(1)} %fusion.55), channel_id=1, replica_groups=mesh['tp'=4,'dp'=8] {'dp'}, dimensions={0}, use_global_device_ids=true | all-gather | bytes 73728 | tf_op jit(solution)/shard_map/all_gather | solution.py:123
  107.0 2.0 fusion.22
  109.0 16.0 %psum.29 = bf16[16,512]{1,0:T(8,128)(2,1)S(1)} all-reduce(bf16[16,512]{1,0:T(8,128)(2,1)S(1)} %fusion.22), channel_id=1, replica_groups=mesh['tp'=4,'dp'=8] {'tp'}, use_global_device_ids=true, to_apply=%region_9.10 | all-reduce | flops 8192 | bytes 32768 | tf_op jit(solution)/shard_map/psum | solution.py:127
  125.0 2.6 convolution_convert_fusion.1
  127.6 2.6 convolution_convert_fusion
  131.0 26.4 %all-reduce.8 = (bf16[16]{0:T(256)(128)(2,1)S(1)}, bf16[16,1024]{1,0:T(8,128)(2,1)S(1)}, bf16[16,32]{1,0:T(8,128)(2,1)S(1)}) all-reduce(bf16[16]{0:T(256)(128)(2,1)S(1)} %multiply_reduce_fusion.4, bf16[16,1024]{1,0:T(8,128)(2,1)S(1)} %convolution_convert_fusion.4, ...), channel_id=1, replica_groups=mesh['tp'=4,'dp'=8] {'dp'}, use_global_device_ids=true, to_apply=%region_12.13 | all-reduce | flops 16912 | bytes 67648 | tf_op jit(solution)/shard_map/psum | solution.py:63
  158.1 0.7 pad_maximum_fusion.4
  158.7 50.9 %all-reduce.15.cloned.1.call-done = (bf16[16,2048]{1,0:T(8,128)(2,1)}, bf16[16,2048]{1,0:T(8,128)(2,1)}) async-done(((bf16[16,2048]{1,0:T(8,128)(2,1)}, bf16[16,2048]{1,0:T(8,128)(2,1)}), (bf16[16,2048]{1,0:T(8,128)(2,1)}, bf16[16,2048]{1,0:T(8,128)(2,1)})) %all-reduce.15.cloned.1.call-update) | async-done | bytes 131088
  209.7 0.8 fusion.59
  211.0 5.0 %multiply_add_fusion.1 = (f32[1,2,32,64,128]{4,3,2,1,0:T(8,128)S(1)}, f32[1,2,32,64,128]{4,3,2,1,0:T(8,128)}, f32[1,2,32,64,128]{4,3,2,1,0:T(8,128)S(1)}) fusion(f32[2,32,128]{2,1,0:T(8,128)S(1)} %copy-done.5, f32[2,32,64]{2,1,0:T(8,128)S(1)} %multiply_multiply_fusion.1, f32[2,32]{1,0:T(2,128)} %copy-done.18, f32[2,2,32,64,128]{4,3,2,1,0:T(8,128)} %param.29, ...), kind=kLoop, calls=%fused_computation.14 | loop fusion | flops 3145728 | bytes 10584576 | tf_op jit(solution)/shard_map/add | solution.py:109
  216.0 5.2 %fusion.10 = f32[2,4,1,8,64]{4,2,3,1,0:T(1,128)S(1)} fusion(f32[2,4,8,64,128]{4,3,2,1,0:T(8,128)S(1)} %bitcast.139, f32[2,4,128]{2,1,0:T(4,128)S(1)} %bitcast.151, f32[2,4,8,64]{3,2,1,0:T(8,128)S(1)} %broadcast_multiply_fusion, f32[2,4,8]{2,1,0:T(4,128)S(1)} %mul.475, f32[2,2,512]{2,1,0:T(2,128)S(1)} %divide_multiply_fusion.2), kind=kOutput, calls=%fused_computation.17 | convolution fusion | flops 7864320 | bytes 2158592 | tf_op jit(solution)/shard_map/sgepn,sgn->sgep/dot_general | solution.py:112
  221.4 0.9 fusion.62
  222.5 14.0 %all-gather.2 = bf16[8,2,2048]{2,1,0:T(2,128)(2,1)S(1)} all-gather(bf16[1,2,2048]{2,1,0:T(2,128)(2,1)S(1)} %fusion.56), channel_id=1, replica_groups=mesh['tp'=4,'dp'=8] {'dp'}, dimensions={0}, use_global_device_ids=true | all-gather | bytes 73728 | tf_op jit(solution)/shard_map/all_gather | solution.py:123
  236.6 2.0 fusion.25
  238.5 16.0 %psum.31 = bf16[16,512]{1,0:T(8,128)(2,1)S(1)} all-reduce(bf16[16,512]{1,0:T(8,128)(2,1)S(1)} %fusion.25), channel_id=1, replica_groups=mesh['tp'=4,'dp'=8] {'tp'}, use_global_device_ids=true, to_apply=%region_19.20 | all-reduce | flops 8192 | bytes 32768 | tf_op jit(solution)/shard_map/psum | solution.py:127
  254.5 0.6 fusion.57
  255.1 4.0 %pad_maximum_fusion = f32[2,2,32,64,128]{4,3,2,1,0:T(8,128)} fusion(f32[1,2,32,64,128]{4,3,2,1,0:T(8,128)} %get-tuple-element.27, f32[1,2,32,64,128]{4,3,2,1,0:T(8,128)S(1)} %get-tuple-element.26), kind=kLoop, calls=%fused_computation | loop fusion | flops 1048576 | bytes 8388608 | tf_op jit(solution)/shard_map/stack | solution.py:134
  259.1 0.7 pad_maximum_fusion.3
  (126 shorter events, 5.8 us)
Async XLA Ops:
  7.2 72.1 %all-reduce.17.cloned.1.call-start = ((), (), s32[]{:S(2)}) async-start(), calls=%async_computation.1 | async-start | bytes 262144
  23.7 186.0 %all-reduce.15.cloned.1.call-start = ((), (), s32[]{:S(2)}) async-start(), calls=%async_computation | async-start | bytes 262144
  23.8 0.7 copy-start.16
  23.8 1.6 copy-start
  27.6 0.9 copy-start.1
  27.6 29.0 %copy-start.30 = (u32[32]{0:T(128)S(1)}, u32[32]{0:T(128)}, u32[]{:S(2)}) copy-start(u32[32]{0:T(128)} %constant.52) | copy-start | bytes 388
  27.6 30.3 %copy-start.14 = (bf16[2,2,4,2,512]{4,3,2,1,0:T(2,128)(2,1)S(1)}, bf16[2,2,4,2,512]{4,3,2,1,0:T(2,128)(2,1)}, u32[]{:S(2)}) copy-start(bf16[2,2,4,2,512]{4,3,2,1,0:T(2,128)(2,1)} %param.31) | copy-start | bytes 98308
  27.6 30.5 %copy-start.28 = (f32[2,32]{1,0:T(2,128)S(1)}, f32[2,32]{1,0:T(2,128)}, u32[]{:S(2)}) copy-start(f32[2,32]{1,0:T(2,128)} %param.25) | copy-start | bytes 772
  27.6 30.5 %copy-start.29 = (f32[2,32]{1,0:T(2,128)S(1)}, f32[2,32]{1,0:T(2,128)}, u32[]{:S(2)}) copy-start(f32[2,32]{1,0:T(2,128)} %param.24) | copy-start | bytes 772
  27.6 32.4 %copy-start.8 = (bf16[2,2,4,2048]{3,2,1,0:T(4,128)(2,1)S(1)}, bf16[2,2,4,2048]{3,2,1,0:T(4,128)(2,1)}, u32[]{:S(2)}) copy-start(bf16[2,2,4,2048]{3,2,1,0:T(4,128)(2,1)} %param.30) | copy-start | bytes 196612
  27.7 32.4 %copy-start.2 = (bf16[2,5,2048]{2,0,1:T(2,128)(2,1)S(1)}, bf16[2,5,2048]{2,0,1:T(2,128)(2,1)}, u32[]{:S(2)}) copy-start(bf16[2,5,2048]{2,0,1:T(2,128)(2,1)} %param.22) | copy-start | bytes 122884
  27.7 33.8 %copy-start.27 = (f32[2,32]{1,0:T(2,128)S(1)}, f32[2,32]{1,0:T(2,128)}, u32[]{:S(2)}) copy-start(f32[2,32]{1,0:T(2,128)} %param.26) | copy-start | bytes 772
  27.7 34.4 %copy-start.17 = (f32[2,2048]{1,0:T(2,128)S(1)}, f32[2,2048]{1,0:T(2,128)}, u32[]{:S(2)}) copy-start(f32[2,2048]{1,0:T(2,128)} %param.27) | copy-start | bytes 49156
  28.6 55.8 %slice-start = ((f32[2,2,32,64,128]{4,3,2,1,0:T(8,128)}), f32[1,2,32,64,128]{4,3,2,1,0:T(8,128)S(1)}, s32[]{:S(2)}) async-start(f32[2,2,32,64,128]{4,3,2,1,0:T(8,128)} %param.29), calls=%async_computation.2 | async-start | bytes 4194304 | tf_op jit(solution)/shard_map/slice | solution.py:105
  56.6 2.2 copy-start.21
  58.0 0.9 copy-start.12
  58.1 7.4 %copy-start.10 = (f32[2,2,512]{2,1,0:T(2,128)}, f32[2,2,512]{2,1,0:T(2,128)S(1)}, u32[]{:S(2)}) copy-start(f32[2,2,512]{2,1,0:T(2,128)S(1)} %divide_multiply_fusion.3) | copy-start | bytes 24580
  58.1 22.0 %copy-start.11 = (f32[2,1,512]{2,1,0:T(1,128)}, f32[2,1,512]{2,1,0:T(1,128)S(1)}, u32[]{:S(2)}) copy-start(f32[2,1,512]{2,1,0:T(1,128)S(1)} %slice.152) | copy-start | bytes 12292
  58.8 0.6 copy-start.19
  58.8 20.4 %copy-start.18 = (f32[2,32]{1,0:T(2,128)}, f32[2,32]{1,0:T(2,128)S(1)}, u32[]{:S(2)}) copy-start(f32[2,32]{1,0:T(2,128)S(1)} %get-tuple-element.24) | copy-start | bytes 772
  60.0 6.3 %copy-start.13 = (bf16[2,1,2,512]{3,2,0,1:T(2,128)(2,1)S(1)}, bf16[2,1,2,512]{3,2,0,1:T(2,128)(2,1)}, u32[]{:S(2)}) copy-start(bf16[2,1,2,512]{3,2,0,1:T(2,128)(2,1)} %copy-done.12) | copy-start | bytes 12292
  60.0 19.2 %copy-start.22 = (f32[2]{0:T(128)S(1)}, f32[2]{0:T(128)}, u32[]{:S(2)}) copy-start(f32[2]{0:T(128)} %copy-done.21) | copy-start | bytes 28
  80.1 0.6 copy-start.3
  90.3 34.6 %copy-start.24 = (f32[1,512]{1,0:T(1,128)S(1)}, f32[1,512]{1,0:T(1,128)}, u32[]{:S(2)}) copy-start(f32[1,512]{1,0:T(1,128)} %get-tuple-element.46) | copy-start | bytes 6148
  125.0 5.3 %copy-start.6 = (f32[2,32,64]{2,1,0:T(8,128)S(1)}, f32[2,32,64]{2,1,0:T(8,128)}, u32[]{:S(2)}) copy-start(f32[2,32,64]{2,1,0:T(8,128)} %reduce_sum.90) | copy-start | bytes 49156
  125.0 5.3 %copy-start.20 = (f32[2,32]{1,0:T(2,128)S(1)}, f32[2,32]{1,0:T(2,128)}, u32[]{:S(2)}) copy-start(f32[2,32]{1,0:T(2,128)} %copy-done.19) | copy-start | bytes 772
  127.6 3.4 %copy-start.4 = (bf16[2,1,2048]{2,1,0:T(2,128)(2,1)S(1)}, bf16[2,1,2048]{2,1,0:T(2,128)(2,1)}, u32[]{:S(2)}) copy-start(bf16[2,1,2048]{2,1,0:T(2,128)(2,1)} %copy-done.3) | copy-start | bytes 24580
  127.6 30.0 %copy-start.7 = (f32[5,2,512]{2,1,0:T(2,128)S(1)}, f32[5,2,512]{2,1,0:T(2,128)}, u32[]{:S(2)}) copy-start(f32[5,2,512]{2,1,0:T(2,128)} %get-tuple-element.41) | copy-start | bytes 61444
  127.6 30.1 %copy-start.25 = (f32[32]{0:T(128)S(1)}, f32[32]{0:T(128)}, u32[]{:S(2)}) copy-start(f32[32]{0:T(128)} %get-tuple-element.49) | copy-start | bytes 388
  127.6 30.2 %copy-start.26 = (f32[32]{0:T(128)S(1)}, f32[32]{0:T(128)}, u32[]{:S(2)}) copy-start(f32[32]{0:T(128)} %get-tuple-element.52) | copy-start | bytes 388
  127.6 30.5 %copy-start.9 = (bf16[1,2,4,2,512]{4,3,2,1,0:T(2,128)(2,1)S(1)}, bf16[1,2,4,2,512]{4,3,2,1,0:T(2,128)(2,1)}, u32[]{:S(2)}) copy-start(bf16[1,2,4,2,512]{4,3,2,1,0:T(2,128)(2,1)} %fusion.53) | copy-start | bytes 49156
  127.6 83.4 %copy-start.5 = (f32[2,32,128]{2,1,0:T(8,128)S(1)}, f32[2,32,128]{2,1,0:T(8,128)}, u32[]{:S(2)}) copy-start(f32[2,32,128]{2,1,0:T(8,128)} %broadcast_bitcast_fusion.1) | copy-start | bytes 98308
  216.0 5.3 %copy-start.23 = (f32[4,8]{1,0:T(4,128)S(1)}, f32[4,8]{1,0:T(4,128)}, u32[]{:S(2)}) copy-start(f32[4,8]{1,0:T(4,128)} %mul.499) | copy-start | bytes 388
  216.0 6.5 %copy-start.15 = (f32[1,2048]{1,0:T(1,128)S(1)}, f32[1,2048]{1,0:T(1,128)}, u32[]{:S(2)}) copy-start(f32[1,2048]{1,0:T(1,128)} %get-tuple-element.43) | copy-start | bytes 24580
Sparse Core Ops, SparseCore 0:
  23.8 55.3 all-reduce.16
  158.2 51.4 all-reduce.14
where the time goes:
time: 268 us; the launch traced here: 267 us
  blocking collectives  124 us (46%)
  waiting for transfers between devices  63.2 us (24%)
  matrix products  26.6 us (10%)
  other arithmetic  20.9 us (8%)
  local copies, waits for them, and re-layouts  16.8 us (6%)
  between operations  15.1 us (6%)
    unnamed x4, waiting for transfers between devices  63.2 us
    psum x2, blocking collectives, shards(): total_sq = lax.psum(part_sq.astype(jnp.bfloat16), 'dp').astype(jnp.float32)  54.1 us
    psum x2, blocking collectives, shards(): summed = lax.psum(terms.astype(jnp.bfloat16), 'tp').astype(jnp.float32)  32 us
    all_gather x2, blocking collectives, shards(): lax.all_gather(mixed_rows, 'dp', axis=0, tiled=True)  28 us
    dot_general x2, matrix products, shards(): jnp.einsum('sgepn,sgn->sgep', state_new, c_part, precision=lax.Precision....  11.3 us
    all_gather x1, blocking collectives, shards(): whole = lax.all_gather(stream, 'tp', axis=0, tiled=True)  9.79 us
  transfers between devices with their start and end apart: 2, of which 2 were waited for; matrix products, arithmetic and copies ran while one was open for 5% of the time, Pallas kernels for 0%

commit v1 on v0

v1 whole, which is shorter than its diff:
```python
import functools

import jax
import jax.numpy as jnp
from jax import lax
from jax.experimental import pallas as pl
from jax.experimental.pallas import tpu as pltpu
from jax.sharding import PartitionSpec as P

EPS = 1e-06
LANES = 128
MESH = pl.DeviceIdType.MESH
F32 = jnp.float32
BF16 = jnp.bfloat16


def silu(v):
    return v / (1.0 + jnp.exp(-v))


def expand(rows, hot):
    hi = rows.astype(BF16)
    lo = (rows - hi.astype(F32)).astype(BF16)
    return jnp.dot(hi, hot, preferred_element_type=F32) + jnp.dot(
        lo, hot, preferred_element_type=F32
    )


def kernel(n, t, head_dim, *refs):
    (
        stream, gain, xw, zw, bcw, stw, cxw, cbw, bias, dlog, skip, ggain, ow, st_in, cx_in, cb_in,
        s_out, st_out, cx_out, cb_out,
        v_h, v_gain, v_xw, v_zw, v_bcw, v_stw, v_cxw, v_cbw, v_bias, v_dlog, v_skip, v_ggain, v_ow,
        v_st, v_cx, v_cb, v_cxo, v_cbo, v_so,
        h32, oldbf, hot, consts, pre_x, pre_b, cols, psend, precv, mix, terms, hrow,
        in_sem, h_send, h_recv, p_send, p_recv, m_send, m_recv, t_send, t_recv, out_sem,
    ) = refs
    dp = lax.axis_index("dp")
    tp = lax.axis_index("tp")
    layers, width = v_gain.shape
    X = v_xw.shape[2]
    B = v_bcw.shape[2]
    half = B // 2
    SD = v_st.shape[1]
    groups = half // v_st.shape[3]
    gw = X // groups
    heads = v_bias.shape[1]
    S = h32.shape[0]
    rows = S // t
    taps = v_cxw.shape[1]
    model_width = n * width
    ZO, BO, SO = X, 2 * X, 2 * X + B
    QO = SO + v_stw.shape[2]
    C = QO + LANES

    loads = {}
    count = [0]

    def load(key, src, dst):
        c = pltpu.make_async_copy(src, dst, in_sem.at[count[0]])
        count[0] += 1
        c.start()
        loads[key] = c

    load("h", stream, v_h.at[tp])
    load("gain", gain, v_gain)
    for l in range(layers):
        load(("xw", l), xw.at[l], v_xw.at[l])
        load(("bcw", l), bcw.at[l], v_bcw.at[l])
        load(("stw", l), stw.at[l], v_stw.at[l])
        load(("zw", l), zw.at[l], v_zw.at[l])
        if l == 0:
            load("bias", bias, v_bias)
            load("dlog", dlog, v_dlog)
            load("skip", skip, v_skip)
            load("cxw", cxw, v_cxw)
            load("cbw", cbw, v_cbw)
            load("cx", cx_in, v_cx)
            load("cb", cb_in, v_cb)
            load("ggain", ggain, v_ggain)
        load(("st", l), st_in.at[l], v_st.at[l])
        load(("ow", l), ow.at[l], v_ow.at[l])

    barrier = pltpu.get_barrier_semaphore()
    for k in range(1, t):
        pl.semaphore_signal(barrier, inc=1, device_id={"tp": lax.rem(tp + k, t)}, device_id_type=MESH)
    for k in range(1, n):
        pl.semaphore_signal(barrier, inc=1, device_id={"dp": lax.rem(dp + k, n)}, device_id_type=MESH)
    pl.semaphore_wait(barrier, t + n - 2)

    def push(axis, me, size, k, src, dst, ssem, rsem):
        c = pltpu.make_async_remote_copy(
            src_ref=src, dst_ref=dst, send_sem=ssem, recv_sem=rsem,
            device_id={axis: lax.rem(me + k, size)}, device_id_type=MESH,
        )
        c.start()
        return c

    sent = []
    hc = [
        push("tp", tp, t, k, stream, v_h.at[tp], h_send.at[k], h_recv.at[k]) for k in range(1, t)
    ]
    sent += hc

    kk = lax.broadcasted_iota(jnp.int32, hot.shape, 0) - tp * heads
    cc = lax.broadcasted_iota(jnp.int32, hot.shape, 1)
    low = kk * head_dim
    hot[...] = jnp.where((cc >= low) & (cc < low + head_dim), 1.0, 0.0).astype(BF16)
    k2 = lax.broadcasted_iota(jnp.int32, (heads, X), 0) * head_dim
    c2 = lax.broadcasted_iota(jnp.int32, (heads, X), 1)
    hot2 = jnp.where((c2 >= k2) & (c2 < k2 + head_dim), 1.0, 0.0).astype(BF16)

    loads["h"].wait()
    for c in hc:
        c.wait_recv()
    h32[...] = jnp.concatenate([v_h[i].astype(F32) for i in range(t)], axis=0)
    loads["gain"].wait()

    outs = []
    for l in range(layers):
        hv = h32[...]
        normed = (hv * v_gain[l : l + 1, :]).astype(BF16)
        sq = jnp.sum(hv * hv, axis=1, keepdims=True)

        def project(w_ref, wide, offset):
            step = min(wide, 512)
            for o in range(0, wide, step):
                p = jnp.dot(normed, w_ref[l, :, o : o + step], preferred_element_type=F32)
                p = p.astype(BF16)
                for d in range(n):
                    psend[l, d, :, offset + o : offset + o + step] = p[d * SD : (d + 1) * SD]

        pieces = []

        def scatter(i, lo, hi):
            for k in range(1, n):
                to = lax.rem(dp + k, n)
                pieces.append(
                    push(
                        "dp", dp, n, k,
                        psend.at[l, to, :, lo:hi], precv.at[l, dp, :, lo:hi],
                        p_send.at[l, i, k], p_recv.at[l, i, k],
                    )
                )

        loads["xw", l].wait()
        project(v_xw, X, 0)
        scatter(0, 0, X)
        loads["zw", l].wait()
        project(v_zw, X, ZO)
        scatter(1, ZO, ZO + X)
        loads["bcw", l].wait()
        loads["stw", l].wait()
        project(v_bcw, B, BO)
        project(v_stw, v_stw.shape[2], SO)
        sqb = jnp.broadcast_to(sq, (S, LANES)).astype(BF16)
        for d in range(n):
            psend[l, d, :, QO:C] = sqb[d * SD : (d + 1) * SD]
        scatter(2, BO, C)
        sent += pieces

        if l == 0:
            loads["bias"].wait()
            loads["dlog"].wait()
            loads["skip"].wait()
            stack = jnp.concatenate([v_bias[...], jnp.exp(v_dlog[...]), v_skip[...]], axis=0)
            consts[...] = expand(stack, hot2)
            for key in ("cxw", "cbw", "cx", "cb", "ggain"):
                loads[key].wait()
            for m in range(layers):
                wx = v_cxw[m].astype(F32)[: taps - 1]
                wb = v_cbw[m].astype(F32)[: taps - 1]
                for s in range(SD):
                    pre_x[m, s : s + 1] = jnp.sum(v_cx[m, s].astype(F32) * wx, axis=0, keepdims=True)
                    pre_b[m, s : s + 1] = jnp.sum(v_cb[m, s].astype(F32) * wb, axis=0, keepdims=True)
        loads["st", l].wait()
        for s in range(SD):
            oldbf[s] = v_st[l, s].astype(BF16)

        for c in pieces:
            c.wait_recv()

        def total(lo, hi):
            acc = psend[l, dp, :, lo:hi].astype(F32)
            for k in range(1, n):
                acc = acc + precv[l, lax.rem(dp + k, n), :, lo:hi].astype(F32)
            return acc

        inv = lax.rsqrt(total(QO, C)[:, :1] / model_width + EPS)
        step_raw = total(SO, QO) * inv
        proj_bc = (total(BO, SO) * inv).astype(BF16).astype(F32)
        proj_x = (total(0, X) * inv).astype(BF16).astype(F32)
        proj_z = (total(ZO, ZO + X) * inv).astype(BF16).astype(F32)
        wx = v_cxw[l].astype(F32)[taps - 1 : taps]
        wb = v_cbw[l].astype(F32)[taps - 1 : taps]
        bc = silu(pre_b[l] + proj_bc * wb)
        b = bc[:, :half]
        c = bc[:, half:]
        x = silu(pre_x[l] + proj_x * wx)
        raw = expand(step_raw, hot[...]) + consts[l : l + 1, :]
        step = jnp.maximum(raw, 0.0) + jnp.log1p(jnp.exp(-jnp.abs(raw)))
        decay = jnp.exp(-step * consts[layers + l : layers + l + 1, :])
        dtx = step * x
        cbf = c.astype(BF16)
        gate = silu(proj_z)
        nd = half // groups
        parts = []
        for g in range(groups):
            sl = slice(g * gw, (g + 1) * gw)
            ns = slice(g * nd, (g + 1) * nd)
            picked = []
            for s in range(SD):
                r = lax.dot_general(
                    cbf[:, ns], oldbf[s, sl, :], (((1,), (1,)), ((), ())),
                    preferred_element_type=F32,
                )
                picked.append(r[s : s + 1])
            oldc = jnp.concatenate(picked, axis=0)
            dot_bc = jnp.sum(b[:, ns] * c[:, ns], axis=1, keepdims=True)
            y = (
                decay[:, sl] * oldc
                + dtx[:, sl] * dot_bc
                + consts[2 * layers + l : 2 * layers + l + 1, sl] * x[:, sl]
            )
            y = y * gate[:, sl]
            y = y * lax.rsqrt(jnp.mean(y * y, axis=1, keepdims=True) + EPS)
            parts.append(y * v_ggain[l : l + 1, sl])
        mix[l, dp] = jnp.concatenate(parts, axis=1).astype(BF16)
        mc = [
            push("dp", dp, n, k, mix.at[l, dp], mix.at[l, dp], m_send.at[l, k], m_recv.at[l, k])
            for k in range(1, n)
        ]
        sent += mc

        stack = jnp.concatenate([decay, dtx, decay, dtx], axis=0)[: 4 * SD]
        cols[...] = stack.T
        for s in range(SD):
            for g in range(groups):
                sl = slice(g * gw, (g + 1) * gw)
                brow = b[s : s + 1, g * nd : (g + 1) * nd]
                v_st[l, s, sl, :] = (
                    v_st[l, s, sl, :] * cols[sl, s : s + 1] + cols[sl, SD + s : SD + s + 1] * brow
                )
        oc = pltpu.make_async_copy(v_st.at[l], st_out.at[l], out_sem.at[l])
        oc.start()
        outs.append(oc)
        for s in range(SD):
            v_cxo[l, s] = jnp.concatenate(
                [v_cx[l, s].astype(F32)[1:], proj_x[s : s + 1]], axis=0
            ).astype(BF16)
            v_cbo[l, s] = jnp.concatenate(
                [v_cb[l, s].astype(F32)[1:], proj_bc[s : s + 1]], axis=0
            ).astype(BF16)

        loads["ow", l].wait()
        for cpy in mc:
            cpy.wait_recv()
        allrows = jnp.concatenate([mix[l, d].astype(F32) for d in range(n)], axis=0).astype(BF16)
        terms[l, tp] = jnp.dot(allrows, v_ow[l], preferred_element_type=F32).astype(BF16)
        tc = [
            push("tp", tp, t, k, terms.at[l, tp], terms.at[l, tp], t_send.at[l, k], t_recv.at[l, k])
            for k in range(1, t)
        ]
        sent += tc
        for cpy in tc:
            cpy.wait_recv()
        acc = terms[l, 0].astype(F32)
        for i in range(1, t):
            acc = acc + terms[l, i].astype(F32)
        new = (h32[...] + acc).astype(BF16).astype(F32)
        if l < layers - 1:
            h32[...] = new
        else:
            for i in range(t):
                hrow[i] = new[i * rows : (i + 1) * rows]

    v_so[...] = hrow[tp].astype(BF16)
    for i, (src, dst) in enumerate(((v_so, s_out), (v_cxo, cx_out), (v_cbo, cb_out))):
        oc = pltpu.make_async_copy(src, dst, out_sem.at[layers + i])
        oc.start()
        outs.append(oc)
    for cpy in sent:
        cpy.wait_send()
    for oc in outs:
        oc.wait()


def shards(n, t, *args):
    (
        stream, norm_gain, x_weight, z_weight, bc_weight, step_weight, conv_x_weight,
        conv_bc_weight, step_bias, decay_log, skip_gain, group_gain, out_weight, scan_state,
        conv_x_state, conv_bc_state,
    ) = args
    layers, width = norm_gain.shape
    X = x_weight.shape[2]
    half = bc_weight.shape[3]
    B = 2 * half
    SD, heads, head_dim, sdim = scan_state.shape[1:]
    H = step_weight.shape[2]
    rows = stream.shape[0]
    S = rows * t
    keep = conv_x_state.shape[2]
    taps = conv_x_weight.shape[1]
    bcw = bc_weight.reshape(layers, width, B)
    cbw = conv_bc_weight.reshape(layers, taps, B)
    cbs = conv_bc_state.reshape(layers, SD, keep, B)
    st = scan_state.reshape(layers, SD, heads * head_dim, sdim)
    ins = (
        stream, norm_gain, x_weight, z_weight, bcw, step_weight, conv_x_weight, cbw, step_bias,
        decay_log, skip_gain, group_gain, out_weight, st, conv_x_state, cbs,
    )
    C = 2 * X + B + H + LANES
    dma = pltpu.SemaphoreType.DMA
    V = pltpu.VMEM
    scratch = [V((t, rows, width), BF16)]
    scratch += [V(a.shape, a.dtype) for a in ins[1:]]
    scratch += [
        V(conv_x_state.shape, BF16),
        V(cbs.shape, BF16),
        V(stream.shape, BF16),
        V((S, width), F32),
        V((SD, X, sdim), BF16),
        V((H, X), BF16),
        V((3 * layers, X), F32),
        V((layers, SD, X), F32),
        V((layers, SD, B), F32),
        V((X, 4 * SD), F32),
        V((layers, n, SD, C), BF16),
        V((layers, n, SD, C), BF16),
        V((layers, n, SD, X), BF16),
        V((layers, t, S, out_weight.shape[2]), BF16),
        V((t, rows, width), F32),
        dma((10 + 6 * layers,)),
        dma((t,)),
        dma((t,)),
        dma((layers, 3, n)),
        dma((layers, 3, n)),
        dma((layers, n)),
        dma((layers, n)),
        dma((layers, t)),
        dma((layers, t)),
        dma((layers + 3,)),
    ]
    any_spec = pl.BlockSpec(memory_space=pl.ANY)
    res = pl.pallas_call(
        functools.partial(kernel, n, t, head_dim),
        out_shape=(
            jax.ShapeDtypeStruct(stream.shape, BF16),
            jax.ShapeDtypeStruct(st.shape, F32),
            jax.ShapeDtypeStruct(conv_x_state.shape, BF16),
            jax.ShapeDtypeStruct(cbs.shape, BF16),
        ),
        in_specs=[any_spec] * len(ins),
        out_specs=[any_spec] * 4,
        scratch_shapes=scratch,
        compiler_params=pltpu.CompilerParams(
            collective_id=0, has_side_effects=True, vmem_limit_bytes=60 * 1024 * 1024
        ),
        name="mixers",
    )(*ins)
    return (
        res[0], res[1].reshape(scan_state.shape), res[2], res[3].reshape(conv_bc_state.shape)
    )


def solution(mesh):
    n, t = mesh.shape["dp"], mesh.shape["tp"]
    in_specs = (
        P("tp", "dp"),
        P(None, "dp"),
        P(None, "dp", "tp"),
        P(None, "dp", "tp"),
        P(None, "dp", None, "tp"),
        P(None, "dp", None),
        P(None, None, "tp"),
        P(None, None, None, "tp"),
        P(None, "tp"),
        P(None, "tp"),
        P(None, "tp"),
        P(None, "tp"),
        P(None, "tp", "dp"),
        P(None, "dp", "tp", None, None),
        P(None, "dp", None, "tp"),
        P(None, "dp", None, None, "tp"),
    )
    out_specs = (
        P("tp", "dp"),
        P(None, "dp", "tp", None, None),
        P(None, "dp", None, "tp"),
        P(None, "dp", None, None, "tp"),
    )
    return jax.shard_map(
        functools.partial(shards, n, t),
        mesh=mesh, in_specs=in_specs, out_specs=out_specs, check_vma=False,
    )
```

time: 268 us -> 56.4 us (0.21)
  blocking collectives: 124 us -> 0 us
  waiting for transfers between devices: 63.2 us -> 0 us
  Pallas kernels: 0 us -> 38.5 us
  matrix products: 26.6 us -> 0 us
  other arithmetic: 20.9 us -> 0 us
  between operations: 15.1 us -> 0.64 us
    psum x4 -> x0, blocking collectives: 86.1 us -> none  [the longest x2 54.1 us: shards(): total_sq = lax.psum(part_sq.astype(jnp.bfloat16), 'dp').astype(jnp.float32)]
    unnamed x4 -> x0, waiting for transfers between devices: 63.2 us -> none
    pallas_call x0 -> x1, Pallas kernels: none -> 38.5 us  [shards(): pl.pallas_call(functools.partial(kernel, n, t, head_dim), out_shape=(jax....]
    all_gather x3 -> x0, blocking collectives: 37.8 us -> none  [the longest x2 28 us: shards(): lax.all_gather(mixed_rows, 'dp', axis=0, tiled=True)]
    dot_general x12 -> x0, matrix products: 26.6 us -> none  [the longest x2 11.3 us: shards(): jnp.einsum('sgepn,sgn->sgep', state_new, c_part, precision=lax.Precision....]
    reshape x2 -> x4, local copies, waits for them, and re-layouts: 0.17 us -> 8.56 us  [the longest x1 4.42 us: shards(): bcw = bc_weight.reshape(layers, width, B)]
    another operation x7 -> x0, other arithmetic: 6.14 us -> none  [the longest x1 4.04 us: shards(): jnp.stack(states_list)]
    add x3 -> x0, other arithmetic: 5.82 us -> none  [the longest x1 4.98 us: shards(): old_state * decay_heads[..., None, None]]
  transfers between devices with their start and end apart: 2 -> 0, of which waited for: 2 -> 0; matrix products, arithmetic and copies ran while one was open for 5% -> 0% of each run, Pallas kernels for 0% -> 0%
where the time goes in v1:
time: 56.4 us; the launch traced here: 55.9 us
  Pallas kernels  38.5 us (68%)
  local copies, waits for them, and re-layouts  16.7 us (30%)
  between operations  0.64 us (1%)
    pallas_call x1, Pallas kernels, shards(): pl.pallas_call(functools.partial(kernel, n, t, head_dim), out_shape=(jax....  38.5 us
    unnamed x6, local copies, waits for them, and re-layouts  8.15 us
    reshape x1, local copies, waits for them, and re-layouts, shards(): bcw = bc_weight.reshape(layers, width, B)  4.42 us
    reshape x1, local copies, waits for them, and re-layouts, shards(): res[3].reshape(conv_bc_state.shape)  1.39 us
    reshape x1, local copies, waits for them, and re-layouts, shards(): cbs = conv_bc_state.reshape(layers, SD, keep, B)  1.38 us
    reshape x1, local copies, waits for them, and re-layouts, shards(): cbw = conv_bc_weight.reshape(layers, taps, B)  1.36 us

profile of v1, /device:TPU:0, one launch (start us, length us, event | category | flops | bytes accessed | tf_op | source)
XLA Modules:
  0.0 55.9 jit_solution(8475812999537966629)
XLA Ops:
  0.6 1.4 %reshape.32.refs_7_ = bf16[2,5,1024]{2,1,0:T(8,128)(2,1)} reshape(bf16[2,5,2,512]{3,2,1,0:T(2,128)(2,1)} %param.23) | data formatting | bytes 40960 | tf_op jit(solution)/shard_map/reshape | solution.py:305
  2.0 1.4 %reshape.29.refs_15_ = bf16[2,2,4,1024]{3,2,1,0:T(4,128)(2,1)} reshape(bf16[2,2,4,2,512]{4,3,2,1,0:T(2,128)(2,1)} %param.31) | data formatting | bytes 65536 | tf_op jit(solution)/shard_map/reshape | solution.py:306
  3.4 1.4 %copy.22.refs_6_ = bf16[2,5,2048]{2,1,0:T(8,128)(2,1)} copy(bf16[2,5,2048]{2,0,1:T(2,128)(2,1)} %param.22) | data formatting | bytes 81920 | tf_op args[6]
  4.8 4.4 %reshape.26.refs_4_ = bf16[2,512,1024]{2,1,0:T(8,128)(2,1)} reshape(bf16[2,512,2,512]{3,2,1,0:T(2,128)(2,1)} %param.20) | data formatting | bytes 4194304 | tf_op jit(solution)/shard_map/reshape | solution.py:304
  9.2 38.5 %mixers.1 = (bf16[4,512]{1,0:T(4,128)(2,1)}, f32[2,2,2048,128]{3,2,1,0:T(8,128)}, bf16[2,2,4,2048]{3,2,1,0:T(4,128)(2,1)}, bf16[2,2,4,1024]{3,2,1,0:T(4,128)(2,1)}) custom-call(bf16[4,512]{1,0:T(4,128)(2,1)} %refs_0_.1, f32[2,512]{1,0:T(2,128)} %refs_1_.1, bf16[2,512,2048]{2,1,0:T(8,128)(2,1)} %refs_2_.1, bf16[2,512,2048]{2,1,0:T(8,128)(2,1)} %refs_3_.1, ...), custom_call_target="tpu_custom_call" | custom-call | tf_op jit(solution)/shard_map/mixers/pallas_call | solution.py:345
  47.8 1.4 %reshape.31 = bf16[2,2,4,2,512]{4,3,2,1,0:T(2,128)(2,1)} reshape(bf16[2,2,4,1024]{3,2,1,0:T(4,128)(2,1)} %get-tuple-element.11) | data formatting | bytes 65536 | tf_op jit(solution)/shard_map/reshape | solution.py:362
  49.2 1.3 %copy.28 = bf16[4,512]{1,0:T(4,128)(2,1)} copy(bf16[4,512]{1,0:T(4,128)(2,1)} %get-tuple-element.16) | data formatting | bytes 8192
  50.4 0.0 copy-start
  50.4 4.8 %copy.29 = f32[2,2,32,64,128]{4,3,2,1,0:T(8,128)} copy(f32[2,2,32,64,128]{4,3,2,1,0:T(8,128)} %bitcast.2) | data formatting | bytes 8388608
  55.3 0.0 copy-done
  55.3 0.6 %copy.30 = bf16[2,2,4,2048]{3,2,1,0:T(4,128)(2,1)} copy(bf16[2,2,4,2048]{3,2,1,0:T(4,128)(2,1)S(1)} %copy-done) | data formatting | bytes 131072
Async XLA Ops:
  50.4 4.8 %copy-start = (bf16[2,2,4,2048]{3,2,1,0:T(4,128)(2,1)S(1)}, bf16[2,2,4,2048]{3,2,1,0:T(4,128)(2,1)}, u32[]{:S(2)}) copy-start(bf16[2,2,4,2048]{3,2,1,0:T(4,128)(2,1)} %get-tuple-element.18) | copy-start | bytes 196612

commit v2 on v1

--- a/solution.py
+++ b/solution.py
@@ -9,6 +9,7 @@
 
 EPS = 1e-06
 LANES = 128
+VMEM_GRANT = 56 * 1024 * 1024
 MESH = pl.DeviceIdType.MESH
 F32 = jnp.float32
 BF16 = jnp.bfloat16
@@ -29,25 +30,26 @@
 def kernel(n, t, head_dim, *refs):
     (
         stream, gain, xw, zw, bcw, stw, cxw, cbw, bias, dlog, skip, ggain, ow, st_in, cx_in, cb_in,
-        s_out, st_out, cx_out, cb_out,
+        v_so, v_st, v_cxo, v_cbo,
         v_h, v_gain, v_xw, v_zw, v_bcw, v_stw, v_cxw, v_cbw, v_bias, v_dlog, v_skip, v_ggain, v_ow,
-        v_st, v_cx, v_cb, v_cxo, v_cbo, v_so,
-        h32, oldbf, hot, consts, pre_x, pre_b, cols, psend, precv, mix, terms, hrow,
-        in_sem, h_send, h_recv, p_send, p_recv, m_send, m_recv, t_send, t_recv, out_sem,
+        v_cx, v_cb,
+        h32, oldbf, hot, spread, consts, pre_x, pre_b, cols, psend, precv, mix, terms, hrow,
+        in_sem, h_send, h_recv, p_send, p_recv, m_send, m_recv, t_send, t_recv,
     ) = refs
     dp = lax.axis_index("dp")
     tp = lax.axis_index("tp")
     layers, width = v_gain.shape
     X = v_xw.shape[2]
-    B = v_bcw.shape[2]
-    half = B // 2
+    half = v_cb.shape[4]
+    B = 2 * half
+    tiles = v_bcw.shape[1]
     SD = v_st.shape[1]
     groups = half // v_st.shape[3]
     gw = X // groups
     heads = v_bias.shape[1]
     S = h32.shape[0]
     rows = S // t
-    taps = v_cxw.shape[1]
+    taps = v_cxw.shape[0]
     model_width = n * width
     ZO, BO, SO = X, 2 * X, 2 * X + B
     QO = SO + v_stw.shape[2]
@@ -66,7 +68,8 @@
     load("gain", gain, v_gain)
     for l in range(layers):
         load(("xw", l), xw.at[l], v_xw.at[l])
-        load(("bcw", l), bcw.at[l], v_bcw.at[l])
+        for j in range(tiles):
+            load(("bcw", l, j), bcw.at[l, :, :, j * LANES : (j + 1) * LANES], v_bcw.at[l, j])
         load(("stw", l), stw.at[l], v_stw.at[l])
         load(("zw", l), zw.at[l], v_zw.at[l])
         if l == 0:
@@ -110,13 +113,16 @@
     c2 = lax.broadcasted_iota(jnp.int32, (heads, X), 1)
     hot2 = jnp.where((c2 >= k2) & (c2 < k2 + head_dim), 1.0, 0.0).astype(BF16)
 
+    i3 = lax.broadcasted_iota(jnp.int32, spread.shape, 0) * 2
+    c3 = lax.broadcasted_iota(jnp.int32, spread.shape, 1)
+    spread[...] = jnp.where(i3 == c3, 1.0, 0.0).astype(BF16)
+
     loads["h"].wait()
     for c in hc:
         c.wait_recv()
     h32[...] = jnp.concatenate([v_h[i].astype(F32) for i in range(t)], axis=0)
     loads["gain"].wait()
 
-    outs = []
     for l in range(layers):
         hv = h32[...]
         normed = (hv * v_gain[l : l + 1, :]).astype(BF16)
@@ -149,9 +155,17 @@
         loads["zw", l].wait()
         project(v_zw, X, ZO)
         scatter(1, ZO, ZO + X)
-        loads["bcw", l].wait()
+        even = jnp.dot(normed, spread[...], preferred_element_type=F32)
+        both = jnp.concatenate([even, pltpu.roll(even, 1, 1)], axis=0).astype(BF16)
+        for j in range(tiles):
+            loads["bcw", l, j].wait()
+            w = v_bcw.at[l, j].reshape(2 * width, LANES)[...]
+            p = jnp.dot(both, w, preferred_element_type=F32).astype(BF16)
+            for d in range(n):
+                o = BO + j * LANES
+                psend[l, d, :, o : o + LANES] = p[d * SD : (d + 1) * SD]
+                psend[l, d, :, o + half : o + half + LANES] = p[S + d * SD : S + (d + 1) * SD]
         loads["stw", l].wait()
-        project(v_bcw, B, BO)
         project(v_stw, v_stw.shape[2], SO)
         sqb = jnp.broadcast_to(sq, (S, LANES)).astype(BF16)
         for d in range(n):
@@ -168,11 +182,14 @@
             for key in ("cxw", "cbw", "cx", "cb", "ggain"):
                 loads[key].wait()
             for m in range(layers):
-                wx = v_cxw[m].astype(F32)[: taps - 1]
-                wb = v_cbw[m].astype(F32)[: taps - 1]
+                wxs = [v_cxw[k].astype(F32)[m : m + 1] for k in range(taps)]
                 for s in range(SD):
-                    pre_x[m, s : s + 1] = jnp.sum(v_cx[m, s].astype(F32) * wx, axis=0, keepdims=True)
-                    pre_b[m, s : s + 1] = jnp.sum(v_cb[m, s].astype(F32) * wb, axis=0, keepdims=True)
+                    old = v_cx[m, s].astype(F32)
+                    pre_x[m, s : s + 1] = sum(old[k : k + 1] * wxs[k] for k in range(taps - 1))
+                    both = sum(
+                        v_cb[m, s, k].astype(F32) * v_cbw[m, k].astype(F32) for k in range(taps - 1)
+                    )
+                    pre_b[m, s : s + 1] = jnp.concatenate([both[:1], both[1:]], axis=1)
         loads["st", l].wait()
         for s in range(SD):
             oldbf[s] = v_st[l, s].astype(BF16)
@@ -191,8 +208,9 @@
         proj_bc = (total(BO, SO) * inv).astype(BF16).astype(F32)
         proj_x = (total(0, X) * inv).astype(BF16).astype(F32)
         proj_z = (total(ZO, ZO + X) * inv).astype(BF16).astype(F32)
-        wx = v_cxw[l].astype(F32)[taps - 1 : taps]
-        wb = v_cbw[l].astype(F32)[taps - 1 : taps]
+        wx = v_cxw[taps - 1].astype(F32)[l : l + 1]
+        wb = v_cbw[l, taps - 1].astype(F32)
+        wb = jnp.concatenate([wb[:1], wb[1:]], axis=1)
         bc = silu(pre_b[l] + proj_bc * wb)
         b = bc[:, :half]
         c = bc[:, half:]
@@ -241,15 +259,14 @@
                 v_st[l, s, sl, :] = (
                     v_st[l, s, sl, :] * cols[sl, s : s + 1] + cols[sl, SD + s : SD + s + 1] * brow
                 )
-        oc = pltpu.make_async_copy(v_st.at[l], st_out.at[l], out_sem.at[l])
-        oc.start()
-        outs.append(oc)
         for s in range(SD):
             v_cxo[l, s] = jnp.concatenate(
                 [v_cx[l, s].astype(F32)[1:], proj_x[s : s + 1]], axis=0
             ).astype(BF16)
-            v_cbo[l, s] = jnp.concatenate(
-                [v_cb[l, s].astype(F32)[1:], proj_bc[s : s + 1]], axis=0
+            for k in range(taps - 2):
+                v_cbo[l, s, k] = v_cb[l, s, k + 1]
+            v_cbo[l, s, taps - 2] = jnp.concatenate(
+                [proj_bc[s : s + 1, :half], proj_bc[s : s + 1, half:]], axis=0
             ).astype(BF16)
 
         loads["ow", l].wait()
@@ -275,14 +292,18 @@
                 hrow[i] = new[i * rows : (i + 1) * rows]
 
     v_so[...] = hrow[tp].astype(BF16)
-    for i, (src, dst) in enumerate(((v_so, s_out), (v_cxo, cx_out), (v_cbo, cb_out))):
-        oc = pltpu.make_async_copy(src, dst, out_sem.at[layers + i])
-        oc.start()
-        outs.append(oc)
     for cpy in sent:
         cpy.wait_send()
-    for oc in outs:
-        oc.wait()
+
+
+def store(*refs):
+    sem = refs[-1]
+    half = (len(refs) - 1) // 2
+    copies = [pltpu.make_async_copy(refs[i], refs[half + i], sem.at[i]) for i in range(half)]
+    for c in copies:
+        c.start()
+    for c in copies:
+        c.wait()
 
 
 def shards(n, t, *args):
@@ -301,26 +322,24 @@
     S = rows * t
     keep = conv_x_state.shape[2]
     taps = conv_x_weight.shape[1]
-    bcw = bc_weight.reshape(layers, width, B)
-    cbw = conv_bc_weight.reshape(layers, taps, B)
-    cbs = conv_bc_state.reshape(layers, SD, keep, B)
+    cxw = jnp.transpose(conv_x_weight, (1, 0, 2))
     st = scan_state.reshape(layers, SD, heads * head_dim, sdim)
     ins = (
-        stream, norm_gain, x_weight, z_weight, bcw, step_weight, conv_x_weight, cbw, step_bias,
-        decay_log, skip_gain, group_gain, out_weight, st, conv_x_state, cbs,
+        stream, norm_gain, x_weight, z_weight, bc_weight, step_weight, cxw, conv_bc_weight, step_bias,
+        decay_log, skip_gain, group_gain, out_weight, st, conv_x_state, conv_bc_state,
     )
     C = 2 * X + B + H + LANES
     dma = pltpu.SemaphoreType.DMA
     V = pltpu.VMEM
     scratch = [V((t, rows, width), BF16)]
-    scratch += [V(a.shape, a.dtype) for a in ins[1:]]
+    shapes = [a.shape for a in ins]
+    shapes[4] = (layers, half // LANES, width, 2, LANES)
+    scratch += [V(shapes[i], ins[i].dtype) for i in range(1, len(ins)) if i != 13]
     scratch += [
-        V(conv_x_state.shape, BF16),
-        V(cbs.shape, BF16),
-        V(stream.shape, BF16),
         V((S, width), F32),
         V((SD, X, sdim), BF16),
         V((H, X), BF16),
+        V((width, 2 * width), BF16),
         V((3 * layers, X), F32),
         V((layers, SD, X), F32),
         V((layers, SD, B), F32),
@@ -330,7 +349,7 @@
         V((layers, n, SD, X), BF16),
         V((layers, t, S, out_weight.shape[2]), BF16),
         V((t, rows, width), F32),
-        dma((10 + 6 * layers,)),
+        dma((10 + (5 + half // LANES) * layers,)),
         dma((t,)),
         dma((t,)),
         dma((layers, 3, n)),
@@ -339,28 +358,32 @@
         dma((layers, n)),
         dma((layers, t)),
         dma((layers, t)),
-        dma((layers + 3,)),
     ]
     any_spec = pl.BlockSpec(memory_space=pl.ANY)
+    vmem_spec = pl.BlockSpec(memory_space=V)
+    outs = (stream, st, conv_x_state, conv_bc_state)
     res = pl.pallas_call(
         functools.partial(kernel, n, t, head_dim),
-        out_shape=(
-            jax.ShapeDtypeStruct(stream.shape, BF16),
-            jax.ShapeDtypeStruct(st.shape, F32),
-            jax.ShapeDtypeStruct(conv_x_state.shape, BF16),
-            jax.ShapeDtypeStruct(cbs.shape, BF16),
-        ),
+        out_shape=tuple(V(a.shape, a.dtype) for a in outs),
         in_specs=[any_spec] * len(ins),
-        out_specs=[any_spec] * 4,
+        out_specs=[vmem_spec] * len(outs),
         scratch_shapes=scratch,
         compiler_params=pltpu.CompilerParams(
-            collective_id=0, has_side_effects=True, vmem_limit_bytes=60 * 1024 * 1024
+            collective_id=0, has_side_effects=True, vmem_limit_bytes=VMEM_GRANT
         ),
         name="mixers",
     )(*ins)
-    return (
-        res[0], res[1].reshape(scan_state.shape), res[2], res[3].reshape(conv_bc_state.shape)
-    )
+    res = [pltpu.with_memory_space_constraint(r, V) for r in res]
+    res = pl.pallas_call(
+        store,
+        out_shape=tuple(jax.ShapeDtypeStruct(a.shape, a.dtype) for a in outs),
+        in_specs=[vmem_spec] * len(outs),
+        out_specs=[any_spec] * len(outs),
+        scratch_shapes=[dma((len(outs),))],
+        compiler_params=pltpu.CompilerParams(vmem_limit_bytes=VMEM_GRANT),
+        name="store",
+    )(*res)
+    return (res[0], res[1].reshape(scan_state.shape), res[2], res[3])
 
 
 def solution(mesh):

time: 56.4 us -> 41.9 us (0.74)
  local copies, waits for them, and re-layouts: 16.7 us -> 0 us
  Pallas kernels: 38.5 us -> 41.1 us
    reshape x4 -> x0, local copies, waits for them, and re-layouts: 8.56 us -> none  [the longest x1 4.42 us: shards(): bcw = bc_weight.reshape(layers, width, B)]
    unnamed x6 -> x0, local copies, waits for them, and re-layouts: 8.15 us -> none
    pallas_call x1 -> x2, Pallas kernels: 38.5 us -> 41.1 us  [the longest x1 39.1 us: shards(): pl.pallas_call(functools.partial(kernel, n, t, head_dim), out_shape=tuple...]
where the time goes in v2:
time: 41.9 us; the launch traced here: 41.8 us
  Pallas kernels  41.1 us (98%)
  between operations  0.65 us (2%)
    pallas_call x1, Pallas kernels, shards(): pl.pallas_call(functools.partial(kernel, n, t, head_dim), out_shape=tuple...  39.1 us
    pallas_call x1, Pallas kernels, shards(): pl.pallas_call(store, out_shape=tuple((jax.ShapeDtypeStruct(a.shape, a.dt...  2.06 us

profile of v2, /device:TPU:0, one launch (start us, length us, event | category | flops | bytes accessed | tf_op | source)
XLA Modules:
  0.0 41.8 jit_solution(347415610559509421)
XLA Ops:
  0.6 39.1 %mixers.1 = (bf16[4,512]{1,0:T(4,128)(2,1)S(1)}, f32[2,2,2048,128]{3,2,1,0:T(8,128)S(1)}, bf16[2,2,4,2048]{3,2,1,0:T(4,128)(2,1)S(1)}, bf16[2,2,4,2,512]{4,3,2,1,0:T(2,128)(2,1)S(1)}) custom-call(bf16[4,512]{1,0:T(4,128)(2,1)} %refs_0_.1, f32[2,512]{1,0:T(2,128)} %refs_1_.1, bf16[2,512,2048]{2,1,0:T(8,128)(2,1)} %refs_2_.1, bf16[2,512,2048]{2,1,0:T(8,128)(2,1)} %refs_3_.1, ...), custom_call_target="tpu_custom_call" | custom-call | tf_op jit(solution)/shard_map/mixers/pallas_call | solution.py:365
  39.7 2.1 %store.1 = (bf16[4,512]{1,0:T(4,128)(2,1)}, f32[2,2,2048,128]{3,2,1,0:T(8,128)}, bf16[2,2,4,2048]{3,2,1,0:T(4,128)(2,1)}, bf16[2,2,4,2,512]{4,3,2,1,0:T(2,128)(2,1)}) custom-call(bf16[4,512]{1,0:T(4,128)(2,1)S(1)} %get-tuple-element.12.refs_0_, f32[2,2,2048,128]{3,2,1,0:T(8,128)S(1)} %get-tuple-element.13.refs_1_, ...), custom_call_target="tpu_custom_call" | custom-call | tf_op jit(solution)/shard_map/store/pallas_call | solution.py:377

commit v3 on v2

--- a/solution.py
+++ b/solution.py
@@ -33,7 +33,7 @@
         v_so, v_st, v_cxo, v_cbo,
         v_h, v_gain, v_xw, v_zw, v_bcw, v_stw, v_cxw, v_cbw, v_bias, v_dlog, v_skip, v_ggain, v_ow,
         v_cx, v_cb,
-        h32, oldbf, hot, spread, consts, pre_x, pre_b, cols, psend, precv, mix, terms, hrow,
+        h32, oldbf, hot, spread, consts, pre_x, pre_b, cols, psend, precv, mix, terms, hrow, lsend, lrecv,
         in_sem, h_send, h_recv, p_send, p_recv, m_send, m_recv, t_send, t_recv,
     ) = refs
     dp = lax.axis_index("dp")
@@ -99,6 +99,36 @@
         c.start()
         return c
 
+    side = dp // max(n // 2, 1)
+
+    def peer(j):
+        up, down = n - 1 - j, j
+        far_up = up - 1 + (up + n - dp - 1) // n
+        far_down = down + 1 - (dp - down - 1 + n) // n
+        return side * far_down + (1 - side) * far_up
+
+    def along(src, dst, ssem, rsem):
+        made = []
+        for j in range(n - 1):
+            to = peer(j)
+            c = pltpu.make_async_remote_copy(
+                src_ref=src(to), dst_ref=dst(dp), send_sem=ssem(j), recv_sem=rsem(dp),
+                device_id={"dp": to}, device_id_type=MESH,
+            )
+            c.start()
+            made.append(c)
+        waits = []
+        for k in range(1, n):
+            come = lax.rem(dp + k, n)
+            waits.append(
+                pltpu.make_async_remote_copy(
+                    src_ref=src(come), dst_ref=dst(come), send_sem=ssem(0), recv_sem=rsem(come),
+                    device_id={"dp": come}, device_id_type=MESH,
+                )
+            )
+        sent.extend(made)
+        return waits
+
     sent = []
     hc = [
         push("tp", tp, t, k, stream, v_h.at[tp], h_send.at[k], h_recv.at[k]) for k in range(1, t)
@@ -139,15 +169,12 @@
         pieces = []
 
         def scatter(i, lo, hi):
-            for k in range(1, n):
-                to = lax.rem(dp + k, n)
-                pieces.append(
-                    push(
-                        "dp", dp, n, k,
-                        psend.at[l, to, :, lo:hi], precv.at[l, dp, :, lo:hi],
-                        p_send.at[l, i, k], p_recv.at[l, i, k],
-                    )
+            pieces.extend(
+                along(
+                    lambda d: psend.at[l, d, :, lo:hi], lambda d: precv.at[l, d, :, lo:hi],
+                    lambda j: p_send.at[l, i, j], lambda d: p_recv.at[l, i, d],
                 )
+            )
 
         loads["xw", l].wait()
         project(v_xw, X, 0)
@@ -171,7 +198,6 @@
         for d in range(n):
             psend[l, d, :, QO:C] = sqb[d * SD : (d + 1) * SD]
         scatter(2, BO, C)
-        sent += pieces
 
         if l == 0:
             loads["bias"].wait()
@@ -244,11 +270,10 @@
             y = y * lax.rsqrt(jnp.mean(y * y, axis=1, keepdims=True) + EPS)
             parts.append(y * v_ggain[l : l + 1, sl])
         mix[l, dp] = jnp.concatenate(parts, axis=1).astype(BF16)
-        mc = [
-            push("dp", dp, n, k, mix.at[l, dp], mix.at[l, dp], m_send.at[l, k], m_recv.at[l, k])
-            for k in range(1, n)
-        ]
-        sent += mc
+        mc = along(
+            lambda d: mix.at[l, dp], lambda d: mix.at[l, d],
+            lambda j: m_send.at[l, j], lambda d: m_recv.at[l, d],
+        )
 
         stack = jnp.concatenate([decay, dtx, decay, dtx], axis=0)[: 4 * SD]
         cols[...] = stack.T
@@ -273,25 +298,35 @@
         for cpy in mc:
             cpy.wait_recv()
         allrows = jnp.concatenate([mix[l, d].astype(F32) for d in range(n)], axis=0).astype(BF16)
-        terms[l, tp] = jnp.dot(allrows, v_ow[l], preferred_element_type=F32).astype(BF16)
-        tc = [
-            push("tp", tp, t, k, terms.at[l, tp], terms.at[l, tp], t_send.at[l, k], t_recv.at[l, k])
-            for k in range(1, t)
-        ]
+        term = jnp.dot(allrows, v_ow[l], preferred_element_type=F32).astype(BF16)
+        last = l == layers - 1
+        if last:
+            for i in range(t):
+                lsend[i] = term[i * rows : (i + 1) * rows]
+        else:
+            terms[l, tp] = term
+        tc = []
+        for k in range(1, t):
+            src = lsend.at[lax.rem(tp + k, t)] if last else terms.at[l, tp]
+            dst = lrecv.at[tp] if last else terms.at[l, tp]
+            tc.append(push("tp", tp, t, k, src, dst, t_send.at[l, k], t_recv.at[l, k]))
         sent += tc
+        if last:
+            for i in range(t):
+                hrow[i] = h32[i * rows : (i + 1) * rows]
+            acc = lsend[tp].astype(F32)
         for cpy in tc:
             cpy.wait_recv()
-        acc = terms[l, 0].astype(F32)
-        for i in range(1, t):
-            acc = acc + terms[l, i].astype(F32)
-        new = (h32[...] + acc).astype(BF16).astype(F32)
-        if l < layers - 1:
-            h32[...] = new
+        if last:
+            for k in range(1, t):
+                acc = acc + lrecv[lax.rem(tp + k, t)].astype(F32)
+            v_so[...] = (hrow[tp] + acc).astype(BF16)
         else:
-            for i in range(t):
-                hrow[i] = new[i * rows : (i + 1) * rows]
-
-    v_so[...] = hrow[tp].astype(BF16)
+            acc = terms[l, 0].astype(F32)
+            for i in range(1, t):
+                acc = acc + terms[l, i].astype(F32)
+            h32[...] = (h32[...] + acc).astype(BF16).astype(F32)
+
     for cpy in sent:
         cpy.wait_send()
 
@@ -349,6 +384,8 @@
         V((layers, n, SD, X), BF16),
         V((layers, t, S, out_weight.shape[2]), BF16),
         V((t, rows, width), F32),
+        V((t, rows, width), BF16),
+        V((t, rows, width), BF16),
         dma((10 + (5 + half // LANES) * layers,)),
         dma((t,)),
         dma((t,)),

time: 41.9 us -> 41.4 us (0.988)
  Pallas kernels: 41.1 us -> 40.6 us
    pallas_call x1, Pallas kernels: 39.1 us -> 38.6 us  [shards(): pl.pallas_call(functools.partial(kernel, n, t, head_dim), out_shape=tuple...]
where the time goes in v3:
time: 41.4 us; the launch traced here: 41.3 us
  Pallas kernels  40.6 us (98%)
  between operations  0.65 us (2%)
    pallas_call x1, Pallas kernels, shards(): pl.pallas_call(functools.partial(kernel, n, t, head_dim), out_shape=tuple...  38.6 us
    pallas_call x1, Pallas kernels, shards(): pl.pallas_call(store, out_shape=tuple((jax.ShapeDtypeStruct(a.shape, a.dt...  2.06 us

profile of v3, /device:TPU:0, one launch (start us, length us, event | category | flops | bytes accessed | tf_op | source)
XLA Modules:
  0.0 41.3 jit_solution(4852036137355265270)
XLA Ops:
  0.6 38.6 %mixers.1 = (bf16[4,512]{1,0:T(4,128)(2,1)S(1)}, f32[2,2,2048,128]{3,2,1,0:T(8,128)S(1)}, bf16[2,2,4,2048]{3,2,1,0:T(4,128)(2,1)S(1)}, bf16[2,2,4,2,512]{4,3,2,1,0:T(2,128)(2,1)S(1)}) custom-call(bf16[4,512]{1,0:T(4,128)(2,1)} %refs_0_.1, f32[2,512]{1,0:T(2,128)} %refs_1_.1, bf16[2,512,2048]{2,1,0:T(8,128)(2,1)} %refs_2_.1, bf16[2,512,2048]{2,1,0:T(8,128)(2,1)} %refs_3_.1, ...), custom_call_target="tpu_custom_call" | custom-call | tf_op jit(solution)/shard_map/mixers/pallas_call | solution.py:402
  39.2 2.1 %store.1 = (bf16[4,512]{1,0:T(4,128)(2,1)}, f32[2,2,2048,128]{3,2,1,0:T(8,128)}, bf16[2,2,4,2048]{3,2,1,0:T(4,128)(2,1)}, bf16[2,2,4,2,512]{4,3,2,1,0:T(2,128)(2,1)}) custom-call(bf16[4,512]{1,0:T(4,128)(2,1)S(1)} %get-tuple-element.12.refs_0_, f32[2,2,2048,128]{3,2,1,0:T(8,128)S(1)} %get-tuple-element.13.refs_1_, ...), custom_call_target="tpu_custom_call" | custom-call | tf_op jit(solution)/shard_map/store/pallas_call | solution.py:414

commit v4 on v3

--- a/solution.py
+++ b/solution.py
@@ -68,10 +68,10 @@
     load("gain", gain, v_gain)
     for l in range(layers):
         load(("xw", l), xw.at[l], v_xw.at[l])
+        load(("zw", l), zw.at[l], v_zw.at[l])
         for j in range(tiles):
             load(("bcw", l, j), bcw.at[l, :, :, j * LANES : (j + 1) * LANES], v_bcw.at[l, j])
         load(("stw", l), stw.at[l], v_stw.at[l])
-        load(("zw", l), zw.at[l], v_zw.at[l])
         if l == 0:
             load("bias", bias, v_bias)
             load("dlog", dlog, v_dlog)
@@ -220,20 +220,25 @@
         for s in range(SD):
             oldbf[s] = v_st[l, s].astype(BF16)
 
-        for c in pieces:
-            c.wait_recv()
-
         def total(lo, hi):
             acc = psend[l, dp, :, lo:hi].astype(F32)
             for k in range(1, n):
                 acc = acc + precv[l, lax.rem(dp + k, n), :, lo:hi].astype(F32)
             return acc
 
+        for c in pieces[: n - 1]:
+            c.wait_recv()
+        sum_x = total(0, X)
+        for c in pieces[n - 1 : 2 * (n - 1)]:
+            c.wait_recv()
+        sum_z = total(ZO, ZO + X)
+        for c in pieces[2 * (n - 1) :]:
+            c.wait_recv()
         inv = lax.rsqrt(total(QO, C)[:, :1] / model_width + EPS)
         step_raw = total(SO, QO) * inv
         proj_bc = (total(BO, SO) * inv).astype(BF16).astype(F32)
-        proj_x = (total(0, X) * inv).astype(BF16).astype(F32)
-        proj_z = (total(ZO, ZO + X) * inv).astype(BF16).astype(F32)
+        proj_x = (sum_x * inv).astype(BF16).astype(F32)
+        proj_z = (sum_z * inv).astype(BF16).astype(F32)
         wx = v_cxw[taps - 1].astype(F32)[l : l + 1]
         wb = v_cbw[l, taps - 1].astype(F32)
         wb = jnp.concatenate([wb[:1], wb[1:]], axis=1)

time: 41.4 us -> 41.4 us (level)
  no operation moved by 1% of the time
where the time goes in v4:
time: 41.4 us; the launch traced here: 41.3 us
  Pallas kernels  40.6 us (98%)
  between operations  0.65 us (2%)
    pallas_call x1, Pallas kernels, shards(): pl.pallas_call(functools.partial(kernel, n, t, head_dim), out_shape=tuple...  38.6 us
    pallas_call x1, Pallas kernels, shards(): pl.pallas_call(store, out_shape=tuple((jax.ShapeDtypeStruct(a.shape, a.dt...  2.06 us

profile of v4, /device:TPU:0, one launch (start us, length us, event | category | flops | bytes accessed | tf_op | source)
XLA Modules:
  0.0 41.3 jit_solution(17986336654720782817)
XLA Ops:
  0.6 38.6 %mixers.1 = (bf16[4,512]{1,0:T(4,128)(2,1)S(1)}, f32[2,2,2048,128]{3,2,1,0:T(8,128)S(1)}, bf16[2,2,4,2048]{3,2,1,0:T(4,128)(2,1)S(1)}, bf16[2,2,4,2,512]{4,3,2,1,0:T(2,128)(2,1)S(1)}) custom-call(bf16[4,512]{1,0:T(4,128)(2,1)} %refs_0_.1, f32[2,512]{1,0:T(2,128)} %refs_1_.1, bf16[2,512,2048]{2,1,0:T(8,128)(2,1)} %refs_2_.1, bf16[2,512,2048]{2,1,0:T(8,128)(2,1)} %refs_3_.1, ...), custom_call_target="tpu_custom_call" | custom-call | tf_op jit(solution)/shard_map/mixers/pallas_call | solution.py:407
  39.2 2.1 %store.1 = (bf16[4,512]{1,0:T(4,128)(2,1)}, f32[2,2,2048,128]{3,2,1,0:T(8,128)}, bf16[2,2,4,2048]{3,2,1,0:T(4,128)(2,1)}, bf16[2,2,4,2,512]{4,3,2,1,0:T(2,128)(2,1)}) custom-call(bf16[4,512]{1,0:T(4,128)(2,1)S(1)} %get-tuple-element.12.refs_0_, f32[2,2,2048,128]{3,2,1,0:T(8,128)S(1)} %get-tuple-element.13.refs_1_, ...), custom_call_target="tpu_custom_call" | custom-call | tf_op jit(solution)/shard_map/store/pallas_call | solution.py:419
